TPU v7x, 32 devices: a whole 2x2x4 slice. The times are simulated.
32 devices in a mesh: sp: 8 (over z, y), tp: 4 (over x, core).
Axes of the slice: x: 2, y: 2, z: 4, core: 2. Of those that a mesh axis runs over, the one named last changes fastest.
Arguments:
- tokens: bfloat16 [6144, 2048], P('sp'), may hold values from -6 to 6
- input_gain: bfloat16 [2048], replicated, may hold values from 0.099609375 to 1.8984375
- gate_weight: bfloat16 [2048, 2048], P('sp', 'tp'), may hold values from -0.125 to 0.125
- value_weight: bfloat16 [2048, 2048], P('sp', 'tp'), may hold values from -0.125 to 0.125
- inflow_weight: bfloat16 [2048, 4, 128], P('sp', 'tp'), may hold values from -0.125 to 0.125
- readout_weight: bfloat16 [2048, 4, 128], P('sp', 'tp'), may hold values from -0.125 to 0.125
- step_weight: bfloat16 [2048, 2, 32], P('sp', None, 'tp'), may hold values from -0.125 to 0.125
- conv_values: bfloat16 [5, 2048], P(None, 'tp'), may hold values from -2.5 to 2.5
- conv_inflow: bfloat16 [5, 4, 128], P(None, 'tp'), may hold values from -2.5 to 2.5
- conv_readout: bfloat16 [5, 4, 128], P(None, 'tp'), may hold values from -2.5 to 2.5
- log_rate: float32 [2, 6144, 32], P(None, 'sp', 'tp'), may hold values from -20 to 0
- group_gain: bfloat16 [2048], P('tp'), may hold values from 0.099609375 to 1.8984375
- query_weight: bfloat16 [2048, 2048], P('sp', 'tp'), may hold values from -8 to 8
- key_weight: bfloat16 [2048, 512], P('sp', 'tp'), may hold values from -8 to 8
- vector_weight: bfloat16 [2048, 512], P('sp', 'tp'), may hold values from -0.125 to 0.125
- sink_logit: float32 [32], P('tp'), may hold values from 3 to 7
- state_out: bfloat16 [2048, 2048], P('tp', 'sp'), may hold values from -0.125 to 0.125
- window_out: bfloat16 [2048, 2048], P('tp', 'sp'), may hold values from -1 to 1
Outputs:
- mixed: bfloat16 [6144, 2048], P('sp', 'tp')
- log_total: float32 [6144, 32], P('sp', 'tp')
All inputs are finite; a program needn't handle non-finite values.
Results may differ from a plain program's by a relative error of at most 0.015.
The roundings to bfloat16 on the way count: a program that leaves them out, or rounds other values in their place, can miss the bound.
Values may be sent and summed in bfloat16 or wider, within the bound.
A program may use at most 128 MiB of HBM per device.

v0:
```python
import jax
import jax.numpy as jnp
from jax import lax
from jax.sharding import PartitionSpec as P

HEAD_DIM = 64
CONV = 5
SSD_BLOCK = 128
WINDOW = 128
QBLOCK = 256
GRID_W = 64


EPS = 1e-06
ROPE_BASE = 10000.0
HIGH = lax.Precision.HIGH


def entering(value, axis, join, neutral, backward):
    count = lax.axis_size(axis)
    place = lax.axis_index(axis)
    ahead = count - 1 - place if backward else place
    gathered = jax.tree.map(
        lambda a, kind: lax.all_gather(a.astype(kind), axis),
        value,
        jax.tree.map(lambda a: jnp.bfloat16 if a.dtype == jnp.float32 else a.dtype, value),
    )
    state = jax.tree.map(lambda a, e: jnp.zeros_like(a) + jnp.asarray(e, a.dtype), value, neutral)

    def one(hop, state):
        source = count - 1 - hop if backward else hop
        return join(
            state,
            jax.tree.map(
                lambda a, own: lax.dynamic_index_in_dim(a, source, 0, False).astype(own.dtype),
                gathered,
                value,
            ),
        )

    return lax.fori_loop(0, ahead, one, state)


def with_halo(cells, sides, width):
    for axis, dim in sides:
        count = lax.axis_size(axis)
        ends = count - 1
        head = lax.slice_in_dim(cells, 0, width, axis=dim)
        tail = lax.slice_in_dim(cells, cells.shape[dim] - width, cells.shape[dim], axis=dim)
        cells = jnp.concatenate(
            [
                lax.ppermute(tail, axis, [(i, (i + 1) % count) for i in range(ends)]),
                cells,
                lax.ppermute(head, axis, [((i + 1) % count, i) for i in range(ends)]),
            ],
            axis=dim,
        )
    return cells


def rope_pairs(part, angle):
    half = part.shape[-1] // 2
    cosine = jnp.cos(angle)[:, None, :]
    sine = jnp.sin(angle)[:, None, :]
    first = part[..., :half]
    second = part[..., half:]
    return jnp.concatenate(
        [first * cosine - second * sine, second * cosine + first * sine], axis=-1
    )


def axial_rope(heads, positions):
    width = heads.shape[-1]
    quarter = width // 4
    freqs = ROPE_BASE ** (-jnp.arange(quarter).astype(jnp.float32) / quarter)
    row_angle = (positions // GRID_W).astype(jnp.float32)[:, None] * freqs
    col_angle = (positions % GRID_W).astype(jnp.float32)[:, None] * freqs
    half = width // 2
    wide = heads.astype(jnp.float32)
    turned = jnp.concatenate(
        [rope_pairs(wide[..., :half], row_angle), rope_pairs(wide[..., half:], col_angle)], axis=-1
    )
    return turned.astype(jnp.bfloat16)


def block_ssd(state, inputs):
    xdt, decay, inflow, readout = inputs
    length = decay.shape[0]
    heads = xdt.shape[1]
    groups = inflow.shape[1]
    repeat = heads // groups
    cum = jnp.cumsum(decay, axis=0)
    seg = cum[:, None, :] - cum[None, :, :]
    lower = jnp.arange(length)[:, None] >= jnp.arange(length)[None, :]
    weight = jnp.exp(jnp.where(lower[:, :, None], seg, -jnp.inf))
    intersection = jnp.einsum("lgn,sgn->lsg", readout, inflow, preferred_element_type=jnp.float32)
    intersection = jnp.repeat(intersection, repeat, axis=2)
    final_result = jnp.einsum("lsh,shp->lhp", intersection * weight, xdt, precision=HIGH)
    read_heads = jnp.repeat(readout, repeat, axis=1).astype(jnp.float32)
    final_result = final_result + jnp.exp(cum)[:, :, None] * jnp.einsum(
        "lhn,hpn->lhp", read_heads, state, precision=HIGH
    )
    write_heads = jnp.repeat(inflow, repeat, axis=1).astype(jnp.float32)
    to_end = jnp.exp(cum[-1][None, :] - cum)
    fresh = jnp.einsum("shp,shn->hpn", xdt * to_end[:, :, None], write_heads, precision=HIGH)
    return (jnp.exp(cum[-1])[:, None, None] * state + fresh, final_result)


def chain(earlier, later):
    return (earlier[0] + later[0], jnp.exp(later[0])[:, None, None] * earlier[1] + later[1])


def flatten_rows(weight):
    return weight.reshape(weight.shape[0], -1)


def shards(
    tokens,
    input_gain,
    gate_weight,
    value_weight,
    inflow_weight,
    readout_weight,
    step_weight,
    conv_values,
    conv_inflow,
    conv_readout,
    log_rate,
    group_gain,
    query_weight,
    key_weight,
    vector_weight,
    sink_logit,
    state_out,
    window_out,
):
    count = tokens.shape[0]
    offset = lax.axis_index("sp") * count
    seq_total = count * lax.axis_size("sp")
    positions = offset + jnp.arange(count, dtype=jnp.int32)
    heads = step_weight.shape[2]
    groups = inflow_weight.shape[1]
    state_len = inflow_weight.shape[2]
    inner_local = value_weight.shape[1]
    q_count = query_weight.shape[1] // HEAD_DIM
    kv_count = key_weight.shape[1] // HEAD_DIM
    kv_width = key_weight.shape[1]
    wide = tokens.astype(jnp.float32)
    normed = (
        wide
        * lax.rsqrt(jnp.mean(wide * wide, axis=1, keepdims=True) + EPS)
        * input_gain.astype(jnp.float32)
    ).astype(jnp.bfloat16)
    out_stack = jnp.concatenate([state_out, window_out], axis=0)
    matrices = (
        lax.all_gather(gate_weight, "sp", axis=0, tiled=True),
        jnp.concatenate(
            [
                lax.all_gather(value_weight, "sp", axis=0, tiled=True),
                flatten_rows(lax.all_gather(inflow_weight, "sp", axis=0, tiled=True)),
                flatten_rows(lax.all_gather(readout_weight, "sp", axis=0, tiled=True)),
            ],
            axis=1,
        ),
        flatten_rows(lax.all_gather(step_weight, "sp", axis=0, tiled=True)),
        lax.all_gather(query_weight, "sp", axis=0, tiled=True),
        jnp.concatenate(
            [
                lax.all_gather(key_weight, "sp", axis=0, tiled=True),
                lax.all_gather(vector_weight, "sp", axis=0, tiled=True),
            ],
            axis=1,
        ),
    )
    sums = tuple(
        (jnp.dot(normed, matrix, preferred_element_type=jnp.float32) for matrix in matrices)
    )
    gate = sums[0].astype(jnp.bfloat16)
    conv_input = sums[1].astype(jnp.bfloat16)
    step = jax.nn.softplus(sums[2]).reshape(count, 2, heads)
    queries = sums[3].astype(jnp.bfloat16)
    keyvals = sums[4].astype(jnp.bfloat16)

    def direction(xdt, decay, inflow, readout, backward):
        if backward:
            xdt = jnp.flip(xdt, 0)
            decay = jnp.flip(decay, 0)
            inflow = jnp.flip(inflow, 0)
            readout = jnp.flip(readout, 0)
        blocks = count // SSD_BLOCK
        start_state = jnp.zeros((heads, HEAD_DIM, state_len), jnp.float32)
        shaped = (
            xdt.reshape(blocks, SSD_BLOCK, heads, HEAD_DIM),
            decay.reshape(blocks, SSD_BLOCK, heads),
            inflow.reshape(blocks, SSD_BLOCK, groups, state_len),
            readout.reshape(blocks, SSD_BLOCK, groups, state_len),
        )
        end_state, local = lax.scan(block_ssd, start_state, shaped)
        local = local.reshape(count, heads, HEAD_DIM)
        summary = (jnp.sum(decay, axis=0), end_state)
        identity = (jnp.zeros((heads,), jnp.float32), jnp.zeros_like(end_state))
        if backward:
            incoming = entering(summary, "sp", chain, identity, True)
        else:
            incoming = entering(summary, "sp", chain, identity, False)
        reach = jnp.exp(jnp.cumsum(decay, axis=0))
        per_head = jnp.repeat(readout, heads // groups, axis=1).astype(jnp.float32)
        local = local + reach[:, :, None] * jnp.einsum(
            "lhn,hpn->lhp", per_head, incoming[1], precision=HIGH
        )
        if backward:
            local = jnp.flip(local, 0)
        return local

    reach_rows = CONV // 2
    padded = with_halo(conv_input, (("sp", 0),), CONV // 2).astype(jnp.float32)
    taps = jnp.concatenate(
        [conv_values, flatten_rows(conv_inflow), flatten_rows(conv_readout)], axis=1
    ).astype(jnp.float32)
    conv_sum = padded[0:count] * taps[0]
    for tap in range(1, 2 * reach_rows + 1):
        conv_sum = conv_sum + padded[tap : tap + count] * taps[tap]
    conv_short = jax.nn.silu(conv_sum).astype(jnp.bfloat16)
    conv_out = conv_short.astype(jnp.float32)
    split_mid = inner_local + groups * state_len
    xs = conv_out[:, :inner_local].reshape(count, heads, HEAD_DIM)
    inflow = conv_short[:, inner_local:split_mid].reshape(count, groups, state_len)
    readout = conv_short[:, split_mid:].reshape(count, groups, state_len)
    decay = -jnp.exp(log_rate) * jnp.transpose(step, (1, 0, 2))
    forward = direction(xs * step[:, 0, :, None], decay[0], inflow, readout, False)
    backward = direction(xs * step[:, 1, :, None], decay[1], inflow, readout, True)
    combined = (forward + backward).reshape(count, -1) * jax.nn.silu(gate.astype(jnp.float32))
    grouped = combined.reshape(count, groups, -1)
    grouped = grouped * lax.rsqrt(jnp.mean(grouped * grouped, axis=2, keepdims=True) + EPS)
    state_features = (grouped.reshape(count, -1) * group_gain.astype(jnp.float32)).astype(
        jnp.bfloat16
    )
    q_heads = axial_rope(queries.reshape(count, q_count, HEAD_DIM), positions)
    k_heads = axial_rope(keyvals[:, :kv_width].reshape(count, kv_count, HEAD_DIM), positions)
    both = jnp.concatenate([k_heads.reshape(count, -1), keyvals[:, kv_width:]], axis=1)
    beside_all = with_halo(both, (("sp", 0),), WINDOW)
    repeat = q_count // kv_count
    band = QBLOCK + 2 * WINDOW
    sinks = sink_logit.reshape(kv_count, repeat, 1, 1)
    grouped_q = q_heads.reshape(count, kv_count, repeat, HEAD_DIM)

    def attend(index):
        start = index * QBLOCK
        block_q = lax.dynamic_slice_in_dim(grouped_q, start, QBLOCK, 0)
        block_kv = lax.dynamic_slice_in_dim(beside_all, start, band, 0)
        block_k = block_kv[:, :kv_width].reshape(band, kv_count, HEAD_DIM)
        block_v = block_kv[:, kv_width:].reshape(band, kv_count, HEAD_DIM)
        scores = jnp.einsum(
            "qkrd,skd->krqs", block_q, block_k, preferred_element_type=jnp.float32
        ) * HEAD_DIM ** (-0.5)
        query_pos = offset + start + jnp.arange(QBLOCK, dtype=jnp.int32)
        key_pos = offset + start - WINDOW + jnp.arange(band, dtype=jnp.int32)
        valid = (
            (jnp.abs(query_pos[:, None] - key_pos[None, :]) <= WINDOW)
            & (key_pos >= 0)[None, :]
            & (key_pos < seq_total)[None, :]
        )
        scores = jnp.where(valid, scores, -jnp.inf)
        top = jnp.maximum(jnp.max(scores, axis=-1, keepdims=True), sinks)
        expo = jnp.exp(scores - top)
        total = jnp.sum(expo, axis=-1, keepdims=True) + jnp.exp(sinks - top)
        probs = expo.astype(jnp.bfloat16)
        values = jnp.einsum("krqs,skd->qkrd", probs, block_v, preferred_element_type=jnp.float32)
        values = values / jnp.transpose(total, (2, 0, 1, 3))
        logs = jnp.transpose((top + jnp.log(total))[..., 0], (2, 0, 1)).reshape(QBLOCK, -1)
        return (values.astype(jnp.bfloat16).reshape(QBLOCK, -1), logs)

    feats, logs = lax.map(attend, jnp.arange(count // QBLOCK, dtype=jnp.int32))
    window_features = feats.reshape(count, -1)
    log_total = logs.reshape(count, -1)
    features = jnp.concatenate([state_features, window_features], axis=1)
    terms = jnp.dot(
        features,
        lax.all_gather(out_stack, "sp", axis=1, tiled=True),
        preferred_element_type=jnp.float32,
    )
    mixed = lax.psum_scatter(terms.astype(jnp.bfloat16), "tp", scatter_dimension=1, tiled=True)
    return (mixed, log_total)


def solution(mesh):
    placed = (
        P("sp", None),
        P(),
        P("sp", "tp"),
        P("sp", "tp"),
        P("sp", "tp", None),
        P("sp", "tp", None),
        P("sp", None, "tp"),
        P(None, "tp"),
        P(None, "tp", None),
        P(None, "tp", None),
        P(None, "sp", "tp"),
        P("tp"),
        P("sp", "tp"),
        P("sp", "tp"),
        P("sp", "tp"),
        P("tp"),
        P("tp", "sp"),
        P("tp", "sp"),
    )
    return jax.shard_map(
        shards,
        mesh=mesh,
        in_specs=placed,
        out_specs=(P("sp", "tp"), P("sp", "tp")),
        check_vma=False,
    )
```

profile of v0, /device:TPU:0, one launch (start us, length us, event | category | flops | bytes accessed | tf_op | source)
XLA Modules:
  0.0 521.5 jit_solution(9552441976194561802)
XLA Ops:
  11.5 34.3 %all_gather.49 = bf16[2048,1,128]{2,0,1:T(8,128)(2,1)S(1)} all-gather(bf16[256,1,128]{2,0,1:T(8,128)(2,1)S(1)} %copy-done.13), channel_id=1, replica_groups=mesh['sp'=8,'tp'=4] {'sp'}, dimensions={0}, use_global_device_ids=true | all-gather | bytes 589824 | tf_op jit(solution)/shard_map/all_gather | solution.py:160
  45.8 32.6 %all_gather.50 = bf16[2048,1,128]{2,0,1:T(8,128)(2,1)S(1)} all-gather(bf16[256,1,128]{2,0,1:T(8,128)(2,1)S(1)} %copy-done.14), channel_id=1, replica_groups=mesh['sp'=8,'tp'=4] {'sp'}, dimensions={0}, use_global_device_ids=true | all-gather | bytes 589824 | tf_op jit(solution)/shard_map/all_gather | solution.py:161
  78.4 30.8 %all_gather.47 = bf16[2048,2,8]{0,2,1:T(8,128)(2,1)S(1)} all-gather(bf16[256,2,8]{0,2,1:T(8,128)(2,1)S(1)} %copy-done.15), channel_id=1, replica_groups=mesh['sp'=8,'tp'=4] {'sp'}, dimensions={0}, use_global_device_ids=true | all-gather | bytes 73728 | tf_op jit(solution)/shard_map/all_gather | solution.py:165
  113.9 5.2 %fusion.96 = bf16[768,768]{1,0:T(8,128)(2,1)S(1)} fusion(bf16[2048,128]{1,0:T(8,128)(2,1)S(1)} %bitcast.351, bf16[2048,128]{1,0:T(8,128)(2,1)S(1)} %bitcast.350, bf16[2048,512]{1,0:T(8,128)(2,1)} %all-gather.11.cloned.1.call-done, bf16[768,2048]{1,0:T(8,128)(2,1)} %param.28, f32[2048]{0:T(1024)S(1)} %convert_element_type.177, f32[768]{0:T(1024)S(1)} %add_rsqrt_fusion.1), kind=kOutput, calls=%fused_computation.142 | convolution fusion | flops 2432237568 | bytes 7482368 | tf_op jit(solution)/shard_map/dot_general | solution.py:176
  119.1 3.6 collective-permute-start
  124.2 4.1 collective-permute-done.1
  135.6 4.9 rev.15
  143.4 3.6 reverse.6
  148.4 80.3 %while.70 = (s32[]{:T(128)}, f32[8,64,128]{2,1,0:T(8,128)S(1)}, f32[6,128,8,64]{1,0,3,2:T(8,128)}, f32[6,128,8]{2,1,0:T(8,128)}, f32[6,128,8,64]{1,0,3,2:T(8,128...) while((s32[]{:T(128)}, f32[8,64,128]{2,1,0:T(8,128)S(1)}, ...), condition=%wide.region_11.12_spmd.clone, body=%wide.region_9.11_spmd.clone.sunk | while | flops 156188672 | bytes 3768644 | solution.py:198
  153.7 7.7 %dynamic_update_slice.32 = f32[6,128,8,64]{1,0,3,2:T(8,128)} dynamic-update-slice(f32[6,128,8,64]{1,0,3,2:T(8,128)} %get-tuple-element.813, f32[1,128,8,64]{1,0,3,2:T(1,128)S(1)} %bitcast.331, s32[]{:T(128)} %get-tuple-element.811, s32[]{:T(128)} %constant.205.clone.1..sunk.4, s32[]{:T(128)} %constant.205.clone.1..sunk.4, s32[]{:T(128)} %constant.205.clone.1..sunk.4) | dynamic-update-slice | bytes 524292 | tf_op jit(solution)/shard_map/while/body/jit(dynamic_update_index_in_dim)/dynamic_update_slice | solution.py:198
  167.1 7.7 %dynamic_update_slice.32 = f32[6,128,8,64]{1,0,3,2:T(8,128)} dynamic-update-slice(f32[6,128,8,64]{1,0,3,2:T(8,128)} %get-tuple-element.813, f32[1,128,8,64]{1,0,3,2:T(1,128)S(1)} %bitcast.331, s32[]{:T(128)} %get-tuple-element.811, s32[]{:T(128)} %constant.205.clone.1..sunk.4, s32[]{:T(128)} %constant.205.clone.1..sunk.4, s32[]{:T(128)} %constant.205.clone.1..sunk.4) | dynamic-update-slice | bytes 524292 | tf_op jit(solution)/shard_map/while/body/jit(dynamic_update_index_in_dim)/dynamic_update_slice | solution.py:198
  180.5 7.7 %dynamic_update_slice.32 = f32[6,128,8,64]{1,0,3,2:T(8,128)} dynamic-update-slice(f32[6,128,8,64]{1,0,3,2:T(8,128)} %get-tuple-element.813, f32[1,128,8,64]{1,0,3,2:T(1,128)S(1)} %bitcast.331, s32[]{:T(128)} %get-tuple-element.811, s32[]{:T(128)} %constant.205.clone.1..sunk.4, s32[]{:T(128)} %constant.205.clone.1..sunk.4, s32[]{:T(128)} %constant.205.clone.1..sunk.4) | dynamic-update-slice | bytes 524292 | tf_op jit(solution)/shard_map/while/body/jit(dynamic_update_index_in_dim)/dynamic_update_slice | solution.py:198
  193.9 7.7 %dynamic_update_slice.32 = f32[6,128,8,64]{1,0,3,2:T(8,128)} dynamic-update-slice(f32[6,128,8,64]{1,0,3,2:T(8,128)} %get-tuple-element.813, f32[1,128,8,64]{1,0,3,2:T(1,128)S(1)} %bitcast.331, s32[]{:T(128)} %get-tuple-element.811, s32[]{:T(128)} %constant.205.clone.1..sunk.4, s32[]{:T(128)} %constant.205.clone.1..sunk.4, s32[]{:T(128)} %constant.205.clone.1..sunk.4) | dynamic-update-slice | bytes 524292 | tf_op jit(solution)/shard_map/while/body/jit(dynamic_update_index_in_dim)/dynamic_update_slice | solution.py:198
  207.2 7.7 %dynamic_update_slice.32 = f32[6,128,8,64]{1,0,3,2:T(8,128)} dynamic-update-slice(f32[6,128,8,64]{1,0,3,2:T(8,128)} %get-tuple-element.813, f32[1,128,8,64]{1,0,3,2:T(1,128)S(1)} %bitcast.331, s32[]{:T(128)} %get-tuple-element.811, s32[]{:T(128)} %constant.205.clone.1..sunk.4, s32[]{:T(128)} %constant.205.clone.1..sunk.4, s32[]{:T(128)} %constant.205.clone.1..sunk.4) | dynamic-update-slice | bytes 524292 | tf_op jit(solution)/shard_map/while/body/jit(dynamic_update_index_in_dim)/dynamic_update_slice | solution.py:198
  220.6 7.7 %dynamic_update_slice.32 = f32[6,128,8,64]{1,0,3,2:T(8,128)} dynamic-update-slice(f32[6,128,8,64]{1,0,3,2:T(8,128)} %get-tuple-element.813, f32[1,128,8,64]{1,0,3,2:T(1,128)S(1)} %bitcast.331, s32[]{:T(128)} %get-tuple-element.811, s32[]{:T(128)} %constant.205.clone.1..sunk.4, s32[]{:T(128)} %constant.205.clone.1..sunk.4, s32[]{:T(128)} %constant.205.clone.1..sunk.4) | dynamic-update-slice | bytes 524292 | tf_op jit(solution)/shard_map/while/body/jit(dynamic_update_index_in_dim)/dynamic_update_slice | solution.py:198
  234.3 64.5 %while.69 = (s32[]{:T(128)}, f32[8,64,128]{2,1,0:T(8,128)S(1)}, f32[6,128,8,64]{1,0,3,2:T(8,128)S(1)}, f32[6,128,8]{2,1,0:T(8,128)}, f32[6,128,8,64]{1,0,3,2:T(8...) while((s32[]{:T(128)}, f32[8,64,128]{2,1,0:T(8,128)S(1)}, ...), condition=%wide.region_3.4_spmd.clone, body=%wide.region_1.3_spmd.clone.sunk | while | flops 156188672 | bytes 3768644 | solution.py:198
  239.6 5.1 dynamic_update_slice.31
  250.3 5.1 dynamic_update_slice.31
  261.1 5.1 dynamic_update_slice.31
  271.8 5.1 dynamic_update_slice.31
  282.5 5.1 dynamic_update_slice.31
  293.3 5.1 dynamic_update_slice.31
  300.4 32.3 %all_gather.58 = bf16[2048,128]{1,0:T(8,128)(2,1)S(1)} all-gather(bf16[256,128]{1,0:T(8,128)(2,1)} %param.41), channel_id=1, replica_groups=mesh['sp'=8,'tp'=4] {'sp'}, dimensions={0}, use_global_device_ids=true | all-gather | bytes 589824 | tf_op jit(solution)/shard_map/all_gather | solution.py:169
  332.7 32.0 %all_gather.59 = bf16[2048,128]{1,0:T(8,128)(2,1)S(1)} all-gather(bf16[256,128]{1,0:T(8,128)(2,1)} %param.42), channel_id=1, replica_groups=mesh['sp'=8,'tp'=4] {'sp'}, dimensions={0}, use_global_device_ids=true | all-gather | bytes 589824 | tf_op jit(solution)/shard_map/all_gather | solution.py:170
  378.9 22.7 %all-reduce.2 = (bf16[64]{0:T(256)(128)(2,1)S(1)}, bf16[64]{0:T(256)(128)(2,1)S(1)}) all-reduce(bf16[64]{0:T(256)(128)(2,1)S(1)} %dynamic-update-slice.1, bf16[64]{0:T(256)(128)(2,1)S(1)} %dynamic-update-slice), channel_id=4, replica_groups=mesh['sp'=8,'tp'=4] {'sp'}, use_global_device_ids=true, to_apply=%add.1 | all-reduce | flops 128 | bytes 512
  402.0 4.9 convolution_convert_fusion.1
  408.2 33.7 %while.68 = (s32[]{:T(128)}, bf16[3,256,512]{2,1,0:T(8,128)(2,1)}, f32[3,256,8]{1,2,0:T(8,128)}, s32[3]{0:T(128)S(1)}, bf16[1024,256]{0,1:T(8,128)(2,1)S(1)}, /*...) while((s32[]{:T(128)}, bf16[3,256,512]{2,1,0:T(8,128)(2,1)}, ...), condition=%wide.region_21.22_spmd, body=%wide.region_18.21_spmd.sunk | while | flops 280901888 | bytes 32392600 | solution.py:273
  447.7 7.4 %while.67 = (s32[]{:T(128)}, f32[8,64,128]{2,1,0:T(8,128)S(1)}, s32[]{:T(128)}, bf16[8,8]{1,0:T(8,128)(2,1)S(1)}, bf16[8,8,64,128]{3,2,1,0:T(8,128)(2,1)}, /*index=5*/s32[]{:T(128)}, s32[]{:T(128)}, s32[]{:T(128)}, s32[]{:T(128)}) while((s32[]{:T(128)}, f32[8,64,128]{2,1,0:T(8,128)S(1)}, s32[]{:T(128)}, bf16[8,8]{1,0:T(8,128)(2,1)S(1)}, ...), condition=%wide.region_16.17_spmd, body=%wide.region_15.16_spmd.sunk | while | flops 196622 | bytes 655587 | solution.py:41
  458.5 3.4 rev.16
  465.6 5.3 %multiply_reduce_fusion = (f32[768]{0:T(1024)S(1)}, f32[768,512]{0,1:T(8,128)S(1)}) fusion(bf16[2048,512]{1,0:T(8,128)(2,1)} %all-gather.13.cloned.1.call-done, bf16[768,2048]{1,0:T(8,128)(2,1)} %param.28, f32[2048]{0:T(1024)S(1)} %convert_element_type.177, f32[768]{0:T(1024)S(1)} %add_rsqrt_fusion.1, f32[768,8,64]{0,2,1:T(8,128)} %fusion.95), kind=kOutput, calls=%fused_computation.141 | convolution fusion | flops 1620442368 | bytes 8402944 | tf_op jit(solution)/shard_map/dot_general | solution.py:176
  472.0 7.1 %convolution_convert_fusion = bf16[768,2048]{1,0:T(8,128)(2,1)} fusion(bf16[1024,2048]{1,0:T(8,128)(2,1)} %all-gather.17.cloned.1.call-done, bf16[768,512]{0,1:T(8,128)(2,1)S(1)} %copy-done.7, bf16[768,512]{0,1:T(8,128)(2,1)S(1)} %multiply_convert_fusion.1), kind=kOutput, calls=%fused_computation.109 | convolution fusion | flops 3225944064 | bytes 8912896 | tf_op jit(solution)/shard_map/dot_general | solution.py:277
  479.1 35.5 %reduce-scatter.2.cloned.1.call-done = bf16[768,512]{1,0:T(8,128)(2,1)} async-done(((bf16[768,2048]{1,0:T(8,128)(2,1)}), bf16[768,512]{1,0:T(8,128)(2,1)}) %reduce-scatter.2.cloned.1.call-update) | async-done | bytes 786448 | tf_op jit(solution)/shard_map/reduce_scatter | solution.py:282
  (411 shorter events, 163.5 us)
Async XLA Ops:
  7.2 4.3 copy-start.17
  7.2 4.4 copy-start.13
  7.2 38.6 %copy-start.14 = (bf16[256,1,128]{2,0,1:T(8,128)(2,1)S(1)}, bf16[256,1,128]{2,0,1:T(8,128)(2,1)}, u32[]{:S(2)}) copy-start(bf16[256,1,128]{2,0,1:T(8,128)(2,1)} %param.33) | copy-start | bytes 196612
  7.2 106.7 %all-gather.11.cloned.1.call-start = ((), (), s32[]{:S(2)}) async-start(), calls=%async_computation.1 | async-start | bytes 2359296 | tf_op jit(solution)/shard_map/all_gather | solution.py:159
  7.9 70.5 %copy-start.15 = (bf16[256,2,8]{0,2,1:T(8,128)(2,1)S(1)}, bf16[256,2,8]{0,2,1:T(8,128)(2,1)}, u32[]{:S(2)}) copy-start(bf16[256,2,8]{0,2,1:T(8,128)(2,1)} %param.34) | copy-start | bytes 24580
  7.9 101.3 %copy-start.22 = (f32[2,768,8]{1,2,0:T(8,128)S(1)}, f32[2,768,8]{1,2,0:T(8,128)}, u32[]{:S(2)}) copy-start(f32[2,768,8]{1,2,0:T(8,128)} %param.38) | copy-start | bytes 147460
  7.9 394.1 %all-gather.15.cloned.1.call-start = ((), (), s32[]{:S(2)}) async-start(), calls=%async_computation.3 | async-start | bytes 2359296 | tf_op jit(solution)/shard_map/all_gather | solution.py:166
  8.7 438.9 %all-gather.21.cloned.1.call-start = ((), (), s32[]{:S(2)}) async-start(), calls=%async_computation.7 | async-start | bytes 1179648 | tf_op jit(solution)/shard_map/all_gather | solution.py:24
  8.8 100.5 %copy-start.4 = (bf16[768,2048]{1,0:T(8,128)(2,1)S(1)}, bf16[768,2048]{1,0:T(8,128)(2,1)}, u32[]{:S(2)}) copy-start(bf16[768,2048]{1,0:T(8,128)(2,1)} %param.28) | copy-start | bytes 9437188
  112.0 7.1 %copy-start.8 = (f32[768,8]{0,1:T(8,128)}, f32[768,8]{0,1:T(8,128)S(1)}, u32[]{:S(2)}) copy-start(f32[768,8]{0,1:T(8,128)S(1)} %rev.14) | copy-start | bytes 73732
  113.9 10.2 %copy-start.16 = (bf16[5,512]{1,0:T(8,128)(2,1)S(1)}, bf16[5,512]{1,0:T(8,128)(2,1)}, u32[]{:S(2)}) copy-start(bf16[5,512]{1,0:T(8,128)(2,1)} %param.35) | copy-start | bytes 15364
  113.9 10.2 %copy-start.18 = (bf16[5,1,128]{2,0,1:T(8,128)(2,1)S(1)}, bf16[5,1,128]{2,0,1:T(8,128)(2,1)}, u32[]{:S(2)}) copy-start(bf16[5,1,128]{2,0,1:T(8,128)(2,1)} %param.37) | copy-start | bytes 3844
  113.9 10.2 %copy-start.19 = (bf16[5,1,128]{2,0,1:T(8,128)(2,1)S(1)}, bf16[5,1,128]{2,0,1:T(8,128)(2,1)}, u32[]{:S(2)}) copy-start(bf16[5,1,128]{2,0,1:T(8,128)(2,1)} %param.36) | copy-start | bytes 3844
  119.1 5.0 collective-permute-start
  122.8 5.5 %collective-permute-start.1 = (bf16[2,768]{1,0:T(2,128)(2,1)S(1)}, bf16[2,768]{1,0:T(2,128)(2,1)S(1)}, u32[]{:S(2)}, u32[]{:S(2)}) collective-permute-start(bf16[2,768]{1,0:T(2,128)(2,1)S(1)} %get-tuple-element.500), channel_id=1, source_target_pairs={{4,0},{8,4},{12,8},{16,12},{20,16},{24,20},{28,24},{5,1},{9,5},{13... | collective-permute-start | bytes 9224 | tf_op jit(solution)/shard_map/ppermute | solution.py:54
  228.7 5.4 %copy-start.6 = (bf16[6,128,1,128]{3,1,2,0:T(8,128)(2,1)}, bf16[6,128,1,128]{3,1,2,0:T(8,128)(2,1)S(1)}, u32[]{:S(2)}) copy-start(bf16[6,128,1,128]{3,1,2,0:T(8,128)(2,1)S(1)} %get-tuple-element.924) | copy-start | bytes 589828
  231.0 230.9 %all-gather.19.cloned.1.call-start = ((), (), s32[]{:S(2)}) async-start(), calls=%async_computation.6 | async-start | bytes 1179648 | tf_op jit(solution)/shard_map/all_gather | solution.py:24
  298.8 69.1 %copy-start.2 = (f32[6,128,8,64]{1,0,3,2:T(8,128)}, f32[6,128,8,64]{1,0,3,2:T(8,128)S(1)}, u32[]{:S(2)}) copy-start(f32[6,128,8,64]{1,0,3,2:T(8,128)S(1)} %get-tuple-element.308) | copy-start | bytes 4718596
  298.8 69.1 %copy-start.5 = (bf16[6,128,1,128]{3,1,2,0:T(8,128)(2,1)}, bf16[6,128,1,128]{3,1,2,0:T(8,128)(2,1)S(1)}, u32[]{:S(2)}) copy-start(bf16[6,128,1,128]{3,1,2,0:T(8,128)(2,1)S(1)} %get-tuple-element.921) | copy-start | bytes 589828
  299.5 166.0 %all-gather.13.cloned.1.call-start = ((), (), s32[]{:S(2)}) async-start(), calls=%async_computation.2 | async-start | bytes 2359296 | tf_op jit(solution)/shard_map/all_gather | solution.py:156
  300.1 170.9 %all-gather.17.cloned.1.call-start = ((), (), s32[]{:S(2)}) async-start(), calls=%async_computation.4 | async-start | bytes 4718592 | tf_op jit(solution)/shard_map/all_gather | solution.py:279
  367.9 4.6 copy-start.9
  367.9 6.9 %copy-start.12 = (f32[8,6,128]{2,0,1:T(8,128)S(1)}, f32[8,6,128]{2,0,1:T(8,128)}, u32[]{:S(2)}) copy-start(f32[8,6,128]{2,0,1:T(8,128)} %get-tuple-element.511) | copy-start | bytes 73732
  367.9 9.3 %copy-start.24 = (u32[32]{0:T(128)S(1)}, u32[32]{0:T(128)}, u32[]{:S(2)}) copy-start(u32[32]{0:T(128)} %constant.229) | copy-start | bytes 388
  368.0 10.7 %copy-start.21 = (bf16[8]{0:T(256)(128)(2,1)S(1)}, bf16[8]{0:T(256)(128)(2,1)}, u32[]{:S(2)}) copy-start(bf16[8]{0:T(256)(128)(2,1)} %get-tuple-element.512) | copy-start | bytes 52
  368.0 33.8 %copy-start.20 = (bf16[512]{0:T(512)(128)(2,1)S(1)}, bf16[512]{0:T(512)(128)(2,1)}, u32[]{:S(2)}) copy-start(bf16[512]{0:T(512)(128)(2,1)} %param.39) | copy-start | bytes 3076
  368.0 33.8 %copy-start.23 = (f32[8]{0:T(128)S(1)}, f32[8]{0:T(128)}, u32[]{:S(2)}) copy-start(f32[8]{0:T(128)} %param.43) | copy-start | bytes 100
  368.6 33.3 %collective-permute-start.2 = (bf16[128,256]{0,1:T(8,128)(2,1)S(1)}, bf16[128,256]{0,1:T(8,128)(2,1)S(1)}, u32[]{:S(2)}, u32[]{:S(2)}) collective-permute-start(bf16[128,256]{0,1:T(8,128)(2,1)S(1)} %get-tuple-element.505), channel_id=1, source_target_pairs={{0,4},{4,8},{8,12},{12,16},{16,20},{20,24},{24,28},{1,5},{5,9},{9,... | collective-permute-start | bytes 196616 | tf_op jit(solution)/shard_map/ppermute | solution.py:52
  370.3 31.6 %collective-permute-start.3 = (bf16[128,256]{0,1:T(8,128)(2,1)S(1)}, bf16[128,256]{0,1:T(8,128)(2,1)S(1)}, u32[]{:S(2)}, u32[]{:S(2)}) collective-permute-start(bf16[128,256]{0,1:T(8,128)(2,1)S(1)} %get-tuple-element.506), channel_id=1, source_target_pairs={{4,0},{8,4},{12,8},{16,12},{20,16},{24,20},{28,24},{5,1},{9,5},{13... | collective-permute-start | bytes 196616 | tf_op jit(solution)/shard_map/ppermute | solution.py:54
  372.5 142.2 %reduce-scatter.2.cloned.1.call-start = ((), (), s32[]{:S(2)}) async-start(), calls=%async_computation.5 | async-start | bytes 3932160 | tf_op jit(solution)/shard_map/reduce_scatter | solution.py:282
  408.2 36.0 %copy-start.1 = (f32[6,128,8,64]{1,0,3,2:T(8,128)S(1)}, f32[6,128,8,64]{1,0,3,2:T(8,128)}, u32[]{:S(2)}) copy-start(f32[6,128,8,64]{1,0,3,2:T(8,128)} %get-tuple-element.311) | copy-start | bytes 4718596
  445.8 9.4 %copy-start.3 = (f32[768,8,64]{0,2,1:T(8,128)S(1)}, f32[768,8,64]{0,2,1:T(8,128)}, u32[]{:S(2)}) copy-start(f32[768,8,64]{0,2,1:T(8,128)} %reshape.529) | copy-start | bytes 4718596
  (6 other events, 14.5 us)
Sparse Core Ops, SparseCore 0:
  10.1 58.7 all-gather.10
  71.1 49.0 all-gather.14
  231.1 40.2 all-gather.20
  299.7 42.6 all-gather.18
  344.3 49.7 all-gather.12
  396.0 74.0 all-gather.16
  479.2 35.3 reduce-scatter.1
where the time goes:
time: 525 us; the launch traced here: 521 us
  blocking collectives  185 us (35%)
  local copies, waits for them, and re-layouts  166 us (32%)
  matrix products  67.6 us (13%)
  waiting for transfers between devices  41.7 us (8%)
  other arithmetic  34.3 us (7%)
  between operations  15.4 us (3%)
  starting transfers between devices  8.34 us (2%)
    dynamic_update_slice x12, local copies, waits for them, and re-layouts, direction(): end_state, local = lax.scan(block_ssd, start_state, shaped)  76.9 us
    reduce_scatter x1, waiting for transfers between devices, shards(): lax.psum_scatter(terms.astype(jnp.bfloat16), 'tp', scatter_dimension=1, t...  35.5 us
    all_gather x1, blocking collectives, shards(): lax.all_gather(inflow_weight, 'sp', axis=0, tiled=True)  34.3 us
    all_gather x1, blocking collectives, shards(): lax.all_gather(readout_weight, 'sp', axis=0, tiled=True)  32.6 us
    all_gather x1, blocking collectives, shards(): lax.all_gather(key_weight, 'sp', axis=0, tiled=True)  32.3 us
    all_gather x1, blocking collectives, shards(): lax.all_gather(vector_weight, 'sp', axis=0, tiled=True)  32 us
    all_gather x1, blocking collectives, shards(): lax.all_gather(step_weight, 'sp', axis=0, tiled=True)  30.8 us
    unnamed x1, blocking collectives  22.7 us
  transfers between devices with their start and end apart: 11, of which 2 were waited for; matrix products, arithmetic and copies ran while one was open for 49% of the time, Pallas kernels for 0%

commit v1 on v0

v1 whole, which is shorter than its diff:
```python
import jax
import jax.numpy as jnp
from jax import lax
from jax.experimental import pallas as pl
from jax.experimental.pallas import tpu as pltpu
from jax.sharding import PartitionSpec as P


HEAD_DIM = 64
CONV = 5
SSD_BLOCK = 128
WINDOW = 128
GRID_W = 64


EPS = 1e-06
ROPE_BASE = 10000.0
HIGHEST = lax.Precision.HIGHEST
F32 = jnp.float32
BF16 = jnp.bfloat16
PAD = 16


def iota(shape, dim):
    return lax.broadcasted_iota(jnp.int32, shape, dim)


def exact(a, b):
    return jnp.dot(a, b, precision=HIGHEST, preferred_element_type=F32)


def spread(heads):
    shape = (heads, heads * HEAD_DIM)
    return (iota(shape, 1) // HEAD_DIM == iota(shape, 0)).astype(F32)


def inner_t(a, b):
    return lax.dot_general(a, b, (((1,), (1,)), ((), ())), preferred_element_type=F32)


def outer_t(a, b):
    return lax.dot_general(a, b, (((0,), (0,)), ((), ())), preferred_element_type=F32)


def summary_kernel(cells_ref, sd_ref, out_ref):
    count = cells_ref.shape[0]
    heads = sd_ref.shape[1] // 4
    wide = heads * HEAD_DIM
    state = out_ref.shape[1] - PAD
    x = cells_ref[:, :wide].astype(F32)
    writes = cells_ref[:, wide : wide + state]
    expand = spread(heads)
    row = iota((count, count), 0)
    col = iota((count, count), 1)
    for e in range(2):
        step = sd_ref[:, e * heads : (e + 1) * heads]
        decay = sd_ref[:, (2 + e) * heads : (3 + e) * heads]
        span = (col > row) if e == 0 else (col < row)
        rest = exact(span.astype(F32), decay)
        scaled = (x * exact(jnp.exp(rest) * step, expand)).astype(BF16)
        out_ref[e, :state, :] = outer_t(writes, scaled).astype(BF16)
        total = exact(jnp.broadcast_to(jnp.sum(decay, axis=0, keepdims=True), (8, heads)), expand)
        total = total[0:1]
        high = total.astype(BF16).astype(F32)
        place = iota((PAD, wide), 0)
        packed = jnp.where(place == 0, high, jnp.where(place == 1, total - high, 0.0))
        out_ref[e, state:, :] = packed.astype(BF16)


def mixer_kernel(cells_ref, sd_ref, sdt_ref, start_ref, gate_ref, gain_ref, out_ref, back_ref, carry_ref):
    blocks, _, size = sdt_ref.shape
    heads = sd_ref.shape[1] // 4
    wide = heads * HEAD_DIM
    state = start_ref.shape[1]
    expand = spread(heads)
    row = iota((size, size), 0)
    col = iota((size, size), 1)
    lower = (row >= col).astype(F32)
    upper = (row <= col).astype(F32)

    carry_ref[...] = start_ref[1]

    def backward(index, _):
        block = blocks - 1 - index
        rows = pl.ds(pl.multiple_of(block * size, size), size)
        back_ref[block] = carry_ref[...].astype(BF16)
        step = sd_ref[rows, heads : 2 * heads]
        cum = exact(upper, sd_ref[rows, 3 * heads : 4 * heads])
        edge = cum[0:1]
        x = cells_ref[rows, :wide].astype(F32)
        scaled = (x * exact(jnp.exp(edge - cum) * step, expand)).astype(BF16)
        fresh = outer_t(cells_ref[rows, wide : wide + state], scaled)
        fade = exact(jnp.broadcast_to(jnp.exp(edge), (8, heads)), expand)[0:1]
        carry_ref[...] = fade * carry_ref[...] + fresh
        return 0

    lax.fori_loop(0, blocks, backward, 0)
    carry_ref[...] = start_ref[0]

    def forward(block, _):
        rows = pl.ds(pl.multiple_of(block * size, size), size)
        cum_f = exact(lower, sd_ref[rows, 2 * heads : 3 * heads])
        cum_b = exact(upper, sd_ref[rows, 3 * heads : 4 * heads])
        flat = sdt_ref[block]
        step_ft = flat[:heads]
        step_bt = flat[heads : 2 * heads]
        cum_ft = exact(flat[2 * heads : 3 * heads], upper)
        cum_bt = exact(flat[3 * heads :], lower)
        x = cells_ref[rows, :wide]
        writes = cells_ref[rows, wide : wide + state]
        reads = cells_ref[rows, wide + state :]
        cross = inner_t(reads, writes)
        parts = []
        for h in range(heads):
            one = slice(h, h + 1)
            seg = jnp.where(
                row >= col, cum_f[:, one] - cum_ft[one], cum_b[:, one] - cum_bt[one]
            )
            scale = jnp.where(
                row > col,
                step_ft[one],
                jnp.where(row < col, step_bt[one], step_ft[one] + step_bt[one]),
            )
            weight = (cross * jnp.exp(seg) * scale).astype(BF16)
            parts.append(
                jnp.dot(
                    weight, x[:, h * HEAD_DIM : (h + 1) * HEAD_DIM], preferred_element_type=F32
                )
            )
        y = jnp.concatenate(parts, axis=1)
        y = y + exact(jnp.exp(cum_f), expand) * jnp.dot(
            reads, carry_ref[...].astype(BF16), preferred_element_type=F32
        )
        y = y + exact(jnp.exp(cum_b), expand) * jnp.dot(
            reads, back_ref[block], preferred_element_type=F32
        )
        gate = gate_ref[rows, :].astype(F32)
        y = y * (gate * jax.nn.sigmoid(gate))
        y = y * lax.rsqrt(jnp.mean(y * y, axis=1, keepdims=True) + EPS)
        out_ref[rows, :] = (y * gain_ref[...].astype(F32)).astype(BF16)
        edge = cum_f[size - 1 : size]
        step = sd_ref[rows, :heads]
        scaled = (x.astype(F32) * exact(jnp.exp(edge - cum_f) * step, expand)).astype(BF16)
        fade = exact(jnp.broadcast_to(jnp.exp(edge), (8, heads)), expand)[0:1]
        carry_ref[...] = fade * carry_ref[...] + outer_t(writes, scaled)
        return 0

    lax.fori_loop(0, blocks, forward, 0)


def attend_kernel(place_ref, sink_ref, q_ref, kv_ref, turn_ref, swap_ref, out_ref, log_ref, keys_ref):
    count = q_ref.shape[0]
    q_count = q_ref.shape[1] // HEAD_DIM
    kv_width = kv_ref.shape[1] // 2
    repeat = q_count * HEAD_DIM // kv_width
    size = SSD_BLOCK
    band = size + 2 * WINDOW
    swap = swap_ref[...]

    def turned(part, rows):
        swapped = jnp.dot(part, swap, preferred_element_type=F32)
        table = turn_ref[rows, :]
        return (part.astype(F32) * table[:, :HEAD_DIM] + swapped * table[:, HEAD_DIM:]).astype(BF16)

    def prepare(block, _):
        rows = pl.ds(pl.multiple_of(block * size, size), size)
        for g in range(kv_width // HEAD_DIM):
            keys_ref[g, rows, :] = turned(
                kv_ref[rows, g * HEAD_DIM : (g + 1) * HEAD_DIM], rows
            )
        return 0

    lax.fori_loop(0, kv_ref.shape[0] // size, prepare, 0)
    row = iota((size, band), 0)
    col = iota((size, band), 1)
    near = (col >= row) & (col - row <= 2 * WINDOW)
    lane = iota((size, q_count), 1)

    def one(block, _):
        start = pl.multiple_of(block * size, size)
        rows = pl.ds(start, size)
        reach = pl.ds(start, band)
        key_pos = place_ref[0] + start - WINDOW + col
        valid = near & (key_pos >= 0) & (key_pos < place_ref[1])
        logs = jnp.zeros((size, q_count), F32)
        outs = []
        for h in range(q_count):
            g = h // repeat
            query = turned(
                q_ref[rows, h * HEAD_DIM : (h + 1) * HEAD_DIM], pl.ds(start + WINDOW, size)
            )
            scores = inner_t(query, keys_ref[g, reach, :]) * HEAD_DIM ** (-0.5)
            scores = jnp.where(valid, scores, -jnp.inf)
            sink = sink_ref[h]
            top = jnp.maximum(jnp.max(scores, axis=1, keepdims=True), sink)
            expo = jnp.exp(scores - top)
            total = jnp.sum(expo, axis=1, keepdims=True) + jnp.exp(sink - top)
            first = kv_width + g * HEAD_DIM
            values = jnp.dot(
                expo.astype(BF16),
                kv_ref[reach, first : first + HEAD_DIM],
                preferred_element_type=F32,
            )
            outs.append((values / total).astype(BF16))
            logs = jnp.where(lane == h, top + jnp.log(total), logs)
        out_ref[rows, :] = jnp.concatenate(outs, axis=1)
        log_ref[rows, :] = logs
        return 0

    lax.fori_loop(0, count // size, one, 0)


def call(kernel, out_shape, args, scratch=(), scalars=0, flops=10**8):
    vmem = pl.BlockSpec(memory_space=pltpu.VMEM)
    smem = pl.BlockSpec(memory_space=pltpu.SMEM)
    return pl.pallas_call(
        kernel,
        out_shape=out_shape,
        in_specs=[smem] * scalars + [vmem] * (len(args) - scalars),
        out_specs=jax.tree.map(lambda _: vmem, out_shape),
        scratch_shapes=list(scratch),
        cost_estimate=pl.CostEstimate(flops=flops, bytes_accessed=4 * 10**6, transcendentals=0),
        compiler_params=pltpu.CompilerParams(vmem_limit_bytes=40 * 2**20),
    )(*args)


def with_halo(cells, sides, width):
    for axis, dim in sides:
        count = lax.axis_size(axis)
        ends = count - 1
        head = lax.slice_in_dim(cells, 0, width, axis=dim)
        tail = lax.slice_in_dim(cells, cells.shape[dim] - width, cells.shape[dim], axis=dim)
        cells = jnp.concatenate(
            [
                lax.ppermute(tail, axis, [(i, (i + 1) % count) for i in range(ends)]),
                cells,
                lax.ppermute(head, axis, [((i + 1) % count, i) for i in range(ends)]),
            ],
            axis=dim,
        )
    return cells


def flatten_rows(weight):
    return weight.reshape(weight.shape[0], -1)


def shards(
    tokens,
    input_gain,
    gate_weight,
    value_weight,
    inflow_weight,
    readout_weight,
    step_weight,
    conv_values,
    conv_inflow,
    conv_readout,
    log_rate,
    group_gain,
    query_weight,
    key_weight,
    vector_weight,
    sink_logit,
    state_out,
    window_out,
):
    count = tokens.shape[0]
    offset = lax.axis_index("sp") * count
    seq_total = count * lax.axis_size("sp")
    heads = step_weight.shape[2]
    groups = inflow_weight.shape[1]
    state_len = inflow_weight.shape[2]
    inner_local = value_weight.shape[1]
    q_count = query_weight.shape[1] // HEAD_DIM
    kv_count = key_weight.shape[1] // HEAD_DIM
    kv_width = key_weight.shape[1]
    wide = tokens.astype(F32)
    normed = (
        wide
        * lax.rsqrt(jnp.mean(wide * wide, axis=1, keepdims=True) + EPS)
        * input_gain.astype(F32)
    ).astype(BF16)

    def whole(parts):
        return lax.all_gather(jnp.concatenate(parts, axis=1), "sp", axis=0, tiled=True)

    own = (flatten_rows(inflow_weight), flatten_rows(readout_weight), flatten_rows(step_weight))
    first_matrix = whole((value_weight,) + own)
    rest_matrix = whole((key_weight, vector_weight, gate_weight, query_weight))
    first = jnp.dot(normed, first_matrix, preferred_element_type=F32)
    rest = jnp.dot(normed, rest_matrix, preferred_element_type=F32).astype(BF16)
    conv_width = inner_local + 2 * groups * state_len
    conv_input = first[:, :conv_width].astype(BF16)
    step = jax.nn.softplus(first[:, conv_width:])
    keyvals = rest[:, : 2 * kv_width]
    gate = rest[:, 2 * kv_width : 2 * kv_width + inner_local]
    queries = rest[:, 2 * kv_width + inner_local :]

    reach_rows = CONV // 2
    padded = with_halo(conv_input, (("sp", 0),), CONV // 2).astype(F32)
    taps = jnp.concatenate(
        [conv_values, flatten_rows(conv_inflow), flatten_rows(conv_readout)], axis=1
    ).astype(F32)
    conv_sum = padded[0:count] * taps[0]
    for tap in range(1, 2 * reach_rows + 1):
        conv_sum = conv_sum + padded[tap : tap + count] * taps[tap]
    cells = jax.nn.silu(conv_sum).astype(BF16)
    rates = jnp.transpose(log_rate, (1, 0, 2)).reshape(count, 2 * heads)
    sd = jnp.concatenate([step, -jnp.exp(rates) * step], axis=1)
    blocks = count // SSD_BLOCK
    sdt = jnp.transpose(sd.reshape(blocks, SSD_BLOCK, 4 * heads), (0, 2, 1))

    summary = call(
        summary_kernel,
        jax.ShapeDtypeStruct((2, state_len + PAD, inner_local), BF16),
        (cells, sd),
    )
    everyone = lax.all_gather(summary, "sp")
    out_stack, everyone = lax.optimization_barrier(
        (jnp.concatenate([state_out, window_out], axis=0), everyone)
    )
    out_matrix = lax.all_gather(out_stack, "sp", axis=1, tiled=True)
    seats = lax.axis_size("sp")
    place = lax.axis_index("sp")
    totals = everyone[:, :, state_len].astype(F32) + everyone[:, :, state_len + 1].astype(F32)
    seat = jnp.arange(seats)
    starts = []
    for e in range(2):
        ahead = seat < place if e == 0 else seat > place
        between = (seat[None, :] > seat[:, None]) if e == 0 else (seat[None, :] < seat[:, None])
        between = (between & ahead[None, :])[:, :, None]
        fade = jnp.sum(jnp.where(between, totals[None, :, e], 0.0), axis=1)
        fade = jnp.where(ahead[:, None], jnp.exp(fade), 0.0)
        starts.append(jnp.sum(fade[:, None, :] * everyone[:, e, :state_len].astype(F32), axis=0))
    starts = jnp.stack(starts)
    state_features = call(
        mixer_kernel,
        jax.ShapeDtypeStruct((count, inner_local), BF16),
        (cells, sd, sdt, starts, gate, group_gain[None]),
        (
            pltpu.VMEM((blocks, state_len, inner_local), BF16),
            pltpu.VMEM((state_len, inner_local), F32),
        ),
        flops=10**10,
    )

    beside = with_halo(keyvals, (("sp", 0),), WINDOW)
    quarter = HEAD_DIM // 4
    freqs = ROPE_BASE ** (-jnp.arange(quarter).astype(F32) / quarter)
    spots = offset - WINDOW + jnp.arange(count + 2 * WINDOW, dtype=jnp.int32)
    row_angle = (spots // GRID_W).astype(F32)[:, None] * freqs
    col_angle = (spots % GRID_W).astype(F32)[:, None] * freqs
    angles = jnp.concatenate([row_angle, col_angle], axis=1)
    cosine = jnp.cos(angles)
    sine = jnp.sin(angles)

    def doubled(table, sign):
        low = table[:, :quarter]
        high = table[:, quarter:]
        return [sign * low, low, sign * high, high]

    turn = jnp.concatenate(doubled(cosine, 1.0) + doubled(sine, -1.0), axis=1)
    channel = jnp.arange(HEAD_DIM)
    partner = channel + jnp.where(channel % (2 * quarter) < quarter, quarter, -quarter)
    swap = (channel[:, None] == partner[None, :]).astype(BF16)
    limits = jnp.stack([offset, seq_total]).astype(jnp.int32)
    window_features, log_total = call(
        attend_kernel,
        (
            jax.ShapeDtypeStruct((count, q_count * HEAD_DIM), BF16),
            jax.ShapeDtypeStruct((count, q_count), F32),
        ),
        (limits, sink_logit, queries, beside, turn, swap),
        (pltpu.VMEM((kv_count, count + 2 * WINDOW, HEAD_DIM), BF16),),
        scalars=2,
        flops=10**10,
    )
    features = jnp.concatenate([state_features, window_features], axis=1)
    terms = jnp.dot(features, out_matrix, preferred_element_type=F32)
    mixed = lax.psum_scatter(terms.astype(BF16), "tp", scatter_dimension=1, tiled=True)
    return (mixed, log_total)


def solution(mesh):
    placed = (
        P("sp", None),
        P(),
        P("sp", "tp"),
        P("sp", "tp"),
        P("sp", "tp", None),
        P("sp", "tp", None),
        P("sp", None, "tp"),
        P(None, "tp"),
        P(None, "tp", None),
        P(None, "tp", None),
        P(None, "sp", "tp"),
        P("tp"),
        P("sp", "tp"),
        P("sp", "tp"),
        P("sp", "tp"),
        P("tp"),
        P("tp", "sp"),
        P("tp", "sp"),
    )
    return jax.shard_map(
        shards,
        mesh=mesh,
        in_specs=placed,
        out_specs=(P("sp", "tp"), P("sp", "tp")),
        check_vma=False,
    )
```

time: 525 us -> 382 us (0.73)
  waiting for transfers between devices: 41.7 us -> 257 us
  blocking collectives: 185 us -> 0 us
  local copies, waits for them, and re-layouts: 166 us -> 10.3 us
  Pallas kernels: 0 us -> 55.6 us
  matrix products: 67.6 us -> 22.5 us
  other arithmetic: 34.3 us -> 13.3 us
    all_gather x6 -> x4, waiting for transfers between devices: 0.09 us -> 212 us  [the longest x2 145 us: whole(): lax.all_gather(jnp.concatenate(parts, axis=1), 'sp', axis=0, tiled=True)]
    all_gather x5 -> x0, blocking collectives: 162 us -> none  [the longest x1 34.3 us: shards(): lax.all_gather(inflow_weight, 'sp', axis=0, tiled=True)]
    dynamic_update_slice x21 -> x0, local copies, waits for them, and re-layouts: 81.3 us -> none  [the longest x12 76.9 us: direction(): end_state, local = lax.scan(block_ssd, start_state, shaped)]
    pallas_call x0 -> x3, Pallas kernels: none -> 55.6 us  [call(): pl.pallas_call(kernel, out_shape=out_shape, in_specs=[smem] * scalars + [...]
    dot_general x62 -> x3, matrix products: 67.6 us -> 22.5 us  [the longest x1 7.71 us: shards(): rest = jnp.dot(normed, rest_matrix, preferred_element_type=F32).astype(BF16)]
    dynamic_slice x15 -> x0, local copies, waits for them, and re-layouts: 24.4 us -> none  [the longest x12 22.6 us: direction(): end_state, local = lax.scan(block_ssd, start_state, shaped)]
    unnamed x1 -> x0, blocking collectives: 22.7 us -> none
    another operation x34 -> x0, local copies, waits for them, and re-layouts: 15.6 us -> none
  transfers between devices with their start and end apart: 11 -> 9, of which waited for: 2 -> 8; matrix products, arithmetic and copies ran while one was open for 49% -> 6% of each run, Pallas kernels for 0% -> 11%
where the time goes in v1:
time: 382 us; the launch traced here: 381 us
  waiting for transfers between devices  257 us (67%)
  Pallas kernels  55.6 us (15%)
  matrix products  22.5 us (6%)
  between operations  14.2 us (4%)
  other arithmetic  13.3 us (3%)
  local copies, waits for them, and re-layouts  10.3 us (3%)
  starting transfers between devices  8.11 us (2%)
    all_gather x2, waiting for transfers between devices, whole(): lax.all_gather(jnp.concatenate(parts, axis=1), 'sp', axis=0, tiled=True)  145 us
    pallas_call x3, Pallas kernels, call(): pl.pallas_call(kernel, out_shape=out_shape, in_specs=[smem] * scalars + [...  55.6 us
    all_gather x1, waiting for transfers between devices, shards(): everyone = lax.all_gather(summary, 'sp')  50.2 us
    reduce_scatter x1, waiting for transfers between devices, shards(): lax.psum_scatter(terms.astype(BF16), 'tp', scatter_dimension=1, tiled=True)  35.4 us
    all_gather x1, waiting for transfers between devices, shards(): out_matrix = lax.all_gather(out_stack, 'sp', axis=1, tiled=True)  16.8 us
    dot_general x1, matrix products, shards(): rest = jnp.dot(normed, rest_matrix, preferred_element_type=F32).astype(BF16)  7.71 us
  transfers between devices with their start and end apart: 9, of which 8 were waited for; matrix products, arithmetic and copies ran while one was open for 6% of the time, Pallas kernels for 11%

profile of v1, /device:TPU:0, one launch (start us, length us, event | category | flops | bytes accessed | tf_op | source)
XLA Modules:
  0.0 381.1 jit_solution(13738347824184548960)
XLA Ops:
  7.2 0.8 copy.40
  8.0 1.8 pad_maximum_fusion.4
  10.6 1.0 convert_reduce_fusion.3
  11.6 2.6 fusion
  14.2 65.5 %all-gather.6.cloned.1.call-done = bf16[2048,784]{1,0:T(8,128)(2,1)} async-done(((bf16[256,784]{1,0:T(8,128)(2,1)}), bf16[2048,784]{1,0:T(8,128)(2,1)}) %all-gather.6.cloned.1.call-update) | async-done | bytes 3211280 | tf_op jit(solution)/shard_map/all_gather | solution.py:286
  79.7 7.3 %fusion.13 = f32[768,784]{0,1:T(8,128)} fusion(bf16[2048,784]{1,0:T(8,128)(2,1)} %all-gather.6.cloned.1.call-done, bf16[768,2048]{1,0:T(8,128)(2,1)} %param.18, f32[2048]{0:T(1024)S(1)} %convert_element_type.72, f32[768]{0:T(1024)S(1)} %add_rsqrt_fusion), kind=kOutput, calls=%fused_computation.25 | convolution fusion | flops 2472542208 | bytes 8776704 | tf_op jit(solution)/shard_map/dot_general | solution.py:291
  87.0 2.0 copy.41
  89.0 2.5 collective-permute-start
  91.5 1.5 collective-permute-start.1
  93.0 0.8 compare_select_fusion
  94.1 3.2 collective-permute-done.1
  97.6 1.8 multiply_convert_fusion.cells_ref
  99.5 13.5 %shard_map.185 = bf16[2,144,512]{2,1,0:T(8,128)(2,1)} custom-call(bf16[768,768]{1,0:T(8,128)(2,1)S(1)} %multiply_convert_fusion.cells_ref, f32[768,32]{1,0:T(8,128)S(1)} %copy.44.sd_ref), custom_call_target="tpu_custom_call" | custom-call | flops 100000000 | bytes 4000000 | tf_op jit(solution)/shard_map/pallas_call | solution.py:216
  113.1 0.9 pad_maximum_fusion
  114.1 0.8 pad_maximum_fusion.1
  115.0 50.2 %all-gather.12.cloned.1.call-done = bf16[16,144,512]{2,1,0:T(8,128)(2,1)} async-done(((bf16[2,144,512]{2,1,0:T(8,128)(2,1)}), bf16[16,144,512]{2,1,0:T(8,128)(2,1)}) %all-gather.12.cloned.1.call-update) | async-done | bytes 2359312 | tf_op jit(solution)/shard_map/all_gather | solution.py:319
  165.8 1.9 fusion.33
  167.6 1.0 fusion.34
  168.6 1.5 fusion.32
  170.1 2.3 concatenate.38.turn_ref
  172.6 79.8 %all-gather.8.cloned.1.call-done = bf16[2048,1280]{1,0:T(8,128)(2,1)} async-done(((bf16[256,1280]{1,0:T(8,128)(2,1)}), bf16[2048,1280]{1,0:T(8,128)(2,1)}) %all-gather.8.cloned.1.call-update) | async-done | bytes 5242896 | tf_op jit(solution)/shard_map/all_gather | solution.py:286
  252.4 7.7 %convolution_convert_fusion.1 = bf16[768,1280]{1,0:T(8,128)(2,1)S(1)} fusion(bf16[2048,1280]{1,0:T(8,128)(2,1)} %all-gather.8.cloned.1.call-done, bf16[768,2048]{1,0:T(8,128)(2,1)} %param.18, f32[2048]{0:T(1024)S(1)} %convert_element_type.72, f32[768]{0:T(1024)S(1)} %add_rsqrt_fusion), kind=kOutput, calls=%fused_computation.6 | convolution fusion | flops 4033806336 | bytes 10365952 | tf_op jit(solution)/shard_map/dot_general | solution.py:292
  260.1 2.5 collective-permute-start.2
  262.6 1.3 collective-permute-start.3
  264.0 1.8 collective-permute-done.2
  265.8 4.3 %collective-permute-done.3 = bf16[128,256]{1,0:T(8,128)(2,1)S(1)} collective-permute-done((bf16[128,256]{1,0:T(8,128)(2,1)S(1)}, bf16[128,256]{1,0:T(8,128)(2,1)S(1)}, u32[]{:S(2)}, u32[]{:S(2)}) %collective-permute-start.3) | collective-permute-done | bytes 65568 | tf_op jit(solution)/shard_map/ppermute | solution.py:237
  270.2 25.9 %shard_map.187 = (bf16[768,512]{1,0:T(8,128)(2,1)S(1)}, f32[768,8]{1,0:T(8,128)S(1)}) custom-call(s32[2]{0:T(128)S(1)} %pad_add_fusion.place_ref, f32[8]{0:T(128)S(1)} %copy-done, bf16[768,512]{1,0:T(8,128)(2,1)S(1)} %get-tuple-element.28.q_ref, bf16[1024,256]{1,0:T(8,128)(2,1)S(1)} %pad_maximum_fusion.3.kv_ref, f32[1024,128]{1,0:T(8,128)S(1)} %concatenate.38.turn_ref, ...), custom_call_target="tpu_custom_call" | custom-call | flops 10000000000 | bytes 4000000 | tf_op jit(solution)/shard_map/pallas_call | solution.py:216
  297.0 16.1 %shard_map.186 = bf16[768,512]{1,0:T(8,128)(2,1)S(1)} custom-call(bf16[768,768]{1,0:T(8,128)(2,1)S(1)} %multiply_convert_fusion.cells_ref, f32[768,32]{1,0:T(8,128)S(1)} %copy.44.sd_ref, f32[6,32,128]{2,1,0:T(8,128)S(1)} %bitcast.37, f32[2,128,512]{2,1,0:T(8,128)S(1)} %pad_maximum_fusion.2.start_ref, bf16[768,512]{1,0:T(8,128)(2,1)S(1)} %get-tuple-element.27.gate_ref, ...), custom_call_target="tpu_custom_call" | custom-call | flops 10000000000 | bytes 4000000 | tf_op jit(solution)/shard_map/pallas_call | solution.py:216
  313.2 0.9 copy-done.1
  314.1 16.8 %all-gather.10.cloned.1.call-done = bf16[1024,2048]{1,0:T(8,128)(2,1)} async-done(((bf16[1024,256]{1,0:T(8,128)(2,1)}), bf16[1024,2048]{1,0:T(8,128)(2,1)}) %all-gather.10.cloned.1.call-update) | async-done | bytes 4194320 | tf_op jit(solution)/shard_map/all_gather | solution.py:323
  330.9 7.5 %convolution_convert_fusion = bf16[768,2048]{1,0:T(8,128)(2,1)} fusion(bf16[1024,2048]{1,0:T(8,128)(2,1)} %all-gather.10.cloned.1.call-done, bf16[768,512]{1,0:T(8,128)(2,1)S(1)} %get-tuple-element.7, bf16[768,512]{1,0:T(8,128)(2,1)} %copy-done.1), kind=kOutput, calls=%fused_computation.5 | convolution fusion | flops 3225944064 | bytes 8912896 | tf_op jit(solution)/shard_map/dot_general | solution.py:380
  339.2 35.4 %reduce-scatter.2.cloned.1.call-done = bf16[768,512]{1,0:T(8,128)(2,1)} async-done(((bf16[768,2048]{1,0:T(8,128)(2,1)}), bf16[768,512]{1,0:T(8,128)(2,1)}) %reduce-scatter.2.cloned.1.call-update) | async-done | bytes 786448 | tf_op jit(solution)/shard_map/reduce_scatter | solution.py:381
  (67 shorter events, 4.0 us)
Async XLA Ops:
  7.2 72.5 %all-gather.6.cloned.1.call-start = ((), (), s32[]{:S(2)}) async-start(), calls=%async_computation.1 | async-start | bytes 4128768 | tf_op jit(solution)/shard_map/all_gather | solution.py:286
  9.9 155.3 %all-gather.12.cloned.1.call-start = ((), (), s32[]{:S(2)}) async-start(), calls=%async_computation.5 | async-start | bytes 2654208 | tf_op jit(solution)/shard_map/all_gather | solution.py:319
  87.0 6.0 %copy-start.9 = (f32[2,768,8]{1,2,0:T(8,128)S(1)}, f32[2,768,8]{1,2,0:T(8,128)}, u32[]{:S(2)}) copy-start(f32[2,768,8]{1,2,0:T(8,128)} %param.28) | copy-start | bytes 147460
  89.0 5.1 %collective-permute-start = (bf16[2,768]{1,0:T(2,128)(2,1)S(1)}, bf16[2,768]{1,0:T(2,128)(2,1)S(1)}, u32[]{:S(2)}, u32[]{:S(2)}) collective-permute-start(bf16[2,768]{1,0:T(2,128)(2,1)S(1)} %get-tuple-element.31), channel_id=1, source_target_pairs={{0,4},{4,8},{8,12},{12,16},{16,20},{20,24},{24,28},{1,5},{5,9},{9,... | collective-permute-start | bytes 9224 | tf_op jit(solution)/shard_map/ppermute | solution.py:235
  91.5 5.8 %collective-permute-start.1 = (bf16[2,768]{1,0:T(2,128)(2,1)S(1)}, bf16[2,768]{1,0:T(2,128)(2,1)S(1)}, u32[]{:S(2)}, u32[]{:S(2)}) collective-permute-start(bf16[2,768]{1,0:T(2,128)(2,1)S(1)} %get-tuple-element.32), channel_id=1, source_target_pairs={{4,0},{8,4},{12,8},{16,12},{20,16},{24,20},{28,24},{5,1},{9,5},{13... | collective-permute-start | bytes 9224 | tf_op jit(solution)/shard_map/ppermute | solution.py:237
  97.6 15.5 %copy-start.3 = (bf16[256,512]{1,0:T(8,128)(2,1)S(1)}, bf16[256,512]{1,0:T(8,128)(2,1)}, u32[]{:S(2)}) copy-start(bf16[256,512]{1,0:T(8,128)(2,1)} %param.30) | copy-start | bytes 786436
  97.6 15.5 %copy-start.4 = (bf16[256,512]{1,0:T(8,128)(2,1)S(1)}, bf16[256,512]{1,0:T(8,128)(2,1)}, u32[]{:S(2)}) copy-start(bf16[256,512]{1,0:T(8,128)(2,1)} %param.20) | copy-start | bytes 786436
  97.6 15.5 %copy-start.7 = (bf16[256,128]{1,0:T(8,128)(2,1)S(1)}, bf16[256,128]{1,0:T(8,128)(2,1)}, u32[]{:S(2)}) copy-start(bf16[256,128]{1,0:T(8,128)(2,1)} %param.32) | copy-start | bytes 196612
  97.6 15.5 %copy-start.8 = (bf16[256,128]{1,0:T(8,128)(2,1)S(1)}, bf16[256,128]{1,0:T(8,128)(2,1)}, u32[]{:S(2)}) copy-start(bf16[256,128]{1,0:T(8,128)(2,1)} %param.31) | copy-start | bytes 196612
  99.4 14.6 %copy-start.10 = (bf16[512]{0:T(512)(128)(2,1)S(1)}, bf16[512]{0:T(512)(128)(2,1)}, u32[]{:S(2)}) copy-start(bf16[512]{0:T(512)(128)(2,1)} %param.29) | copy-start | bytes 3076
  99.4 14.7 %copy-start.5 = (bf16[512,256]{1,0:T(8,128)(2,1)S(1)}, bf16[512,256]{1,0:T(8,128)(2,1)}, u32[]{:S(2)}) copy-start(bf16[512,256]{1,0:T(8,128)(2,1)} %param.35) | copy-start | bytes 786436
  99.4 14.7 %copy-start.6 = (bf16[512,256]{1,0:T(8,128)(2,1)S(1)}, bf16[512,256]{1,0:T(8,128)(2,1)}, u32[]{:S(2)}) copy-start(bf16[512,256]{1,0:T(8,128)(2,1)} %param.34) | copy-start | bytes 786436
  113.0 139.4 %all-gather.8.cloned.1.call-start = ((), (), s32[]{:S(2)}) async-start(), calls=%async_computation.2 | async-start | bytes 5898240 | tf_op jit(solution)/shard_map/all_gather | solution.py:286
  114.0 216.9 %all-gather.10.cloned.1.call-start = ((), (), s32[]{:S(2)}) async-start(), calls=%async_computation.3 | async-start | bytes 4718592 | tf_op jit(solution)/shard_map/all_gather | solution.py:323
  165.2 209.4 %reduce-scatter.2.cloned.1.call-start = ((), (), s32[]{:S(2)}) async-start(), calls=%async_computation.4 | async-start | bytes 3932160 | tf_op jit(solution)/shard_map/reduce_scatter | solution.py:381
  260.1 5.7 %collective-permute-start.2 = (bf16[128,256]{1,0:T(8,128)(2,1)S(1)}, bf16[128,256]{1,0:T(8,128)(2,1)S(1)}, u32[]{:S(2)}, u32[]{:S(2)}) collective-permute-start(bf16[128,256]{1,0:T(8,128)(2,1)S(1)} %get-tuple-element.29), channel_id=1, source_target_pairs={{0,4},{4,8},{8,12},{12,16},{16,20},{20,24},{24,28},{1,5},{5,9},{9,... | collective-permute-start | bytes 196616 | tf_op jit(solution)/shard_map/ppermute | solution.py:235
  262.6 7.6 %copy-start = (f32[8]{0:T(128)S(1)}, f32[8]{0:T(128)}, u32[]{:S(2)}) copy-start(f32[8]{0:T(128)} %sink_ref.1) | copy-start | bytes 100
  262.6 7.5 %collective-permute-start.3 = (bf16[128,256]{1,0:T(8,128)(2,1)S(1)}, bf16[128,256]{1,0:T(8,128)(2,1)S(1)}, u32[]{:S(2)}, u32[]{:S(2)}) collective-permute-start(bf16[128,256]{1,0:T(8,128)(2,1)S(1)} %get-tuple-element.30), channel_id=1, source_target_pairs={{4,0},{8,4},{12,8},{16,12},{20,16},{24,20},{28,24},{5,1},{9,5},{13... | collective-permute-start | bytes 196616 | tf_op jit(solution)/shard_map/ppermute | solution.py:237
  270.1 25.9 %copy-start.2 = (bf16[16,144,512]{2,1,0:T(8,128)(2,1)S(1)}, bf16[16,144,512]{2,1,0:T(8,128)(2,1)}, u32[]{:S(2)}) copy-start(bf16[16,144,512]{2,1,0:T(8,128)(2,1)} %all-gather.12.cloned.1.call-done) | copy-start | bytes 7077892
  313.2 0.9 copy-start.1
Sparse Core Ops, SparseCore 0:
  10.7 68.9 all-gather.5
  113.1 51.9 all-gather.11
  167.9 84.3 all-gather.7
  254.3 76.5 all-gather.9
  338.5 35.9 reduce-scatter.1
